TPU v7x, 256 devices: a 2x2x32 block of a 4x8x32 slice. The times are simulated.
256 devices in a mesh: grp: 4 (over y, x), ep: 64 (over z, core).
Axes of the slice: x: 2, y: 2, z: 32, core: 2. Of those that a mesh axis runs over, the one named last changes fastest.
The devices are a block of a 4x8x32 slice.
Arguments:
- tokens: bfloat16 [8192, 2048], P(('grp', 'ep')), parts along dimension 0, may hold values from -6 to 6
- routing: int32 [8192, 4], P(('grp', 'ep')), parts along dimension 0, may hold values from 0 to 63, as said below
- gate_weights: float32 [8192, 4], P(('grp', 'ep')), parts along dimension 0, may hold values from 0.05 to 1
- pre_gain: float32 [2048], replicated, may hold values from 0.1 to 1.9
- w_gate: bfloat16 [64, 2048, 512], P('ep'), may hold values from -0.125 to 0.125
- w_up: bfloat16 [64, 2048, 512], P('ep'), may hold values from -0.125 to 0.125
- w_down: bfloat16 [64, 512, 2048], P('ep'), may hold values from -0.25 to 0.25
- post_gain: float32 [2048], replicated, may hold values from 0.1 to 1.9
Outputs:
- mixed_out: bfloat16 [8192, 2048], P(('grp', 'ep')), parts along dimension 0
There are 4 independent parts, one for each index of `grp`. A program takes and returns all parts, laid end to end along the dimension named above; an argument that names none is the same for every part. Nothing has to cross between parts.
Inputs may be any that keep to these rules, and one draw needn't show every extreme that they name: `routing`: each row names 4 different experts of one group (experts g * 8 to g * 8 + 7). The rows of one device name any one expert at most 4 times, and some expert exactly 4 times.
All inputs are finite; a program needn't handle non-finite values.
Results may differ from a plain program's by a relative error of at most 0.0085.
Values may be sent and summed in bfloat16 or wider, within the bound.
A program may use at most 64 MiB of HBM per device.

v0:
```python
import jax
import jax.numpy as jnp
from jax import lax
from jax.sharding import Mesh
from jax.sharding import PartitionSpec as P

EP = ("ep_0", "ep_1")
GRP_EP = ("grp", "ep_0", "ep_1")


epsilon = 1e-06


def cut_along(shard, dim, devices):
    dims = shard.shape
    tiles = shard.reshape(*dims[:dim], devices, dims[dim] // devices, *dims[dim + 1 :])
    return jnp.moveaxis(tiles, dim, 0)


def laid_out(tiles, dim):
    tiles = jnp.moveaxis(tiles, 0, dim)
    dims = tiles.shape
    return tiles.reshape(*dims[:dim], dims[dim] * dims[dim + 1], *dims[dim + 2 :])


def exchange_in_order(tiles, axes, sequence):
    dims = [lax.axis_size(a) for a in axes]
    tiles = tiles.reshape(*dims, *tiles.shape[1:])
    for k in sequence:
        tiles = lax.all_to_all(tiles, axes[k], split_axis=k, concat_axis=k, tiled=True)
    return tiles.reshape(-1, *tiles.shape[len(axes) :])


def exchange_by_chip(shard, groups, sequence, split_dim, concat_dim):
    devices = lax.axis_size(groups[0]) * lax.axis_size(groups[1])
    tiles = cut_along(shard, split_dim, devices)
    return laid_out(exchange_in_order(tiles, groups, sequence), concat_dim)


def normalize(values, gain):
    floats = values.astype(jnp.float32)
    return floats * lax.rsqrt(jnp.mean(floats * floats, axis=-1, keepdims=True) + epsilon) * gain


def apply_expert(rows, w_gate, w_up, w_down):
    gate = jnp.dot(rows, w_gate[0], preferred_element_type=jnp.float32)
    upward = jnp.dot(rows, w_up[0], preferred_element_type=jnp.float32)
    hidden = (jax.nn.silu(gate) * upward).astype(jnp.bfloat16)
    return jnp.dot(hidden, w_down[0], preferred_element_type=jnp.float32).astype(jnp.bfloat16)


def body(tokens, routing, gate_weights, pre_gain, w_gate, w_up, w_down, post_gain):
    normed = normalize(tokens, pre_gain).astype(jnp.bfloat16)
    tok_rows, choices_count = routing.shape
    width = tokens.shape[1]
    devices = lax.axis_size(EP)
    capacity = tok_rows * choices_count * 2 // devices
    flat_expert = routing.reshape(-1)
    one_hot = (flat_expert[:, None] == jnp.arange(devices, dtype=jnp.int32)[None, :]).astype(
        jnp.int32
    )
    ranking = jnp.sum((jnp.cumsum(one_hot, axis=0) - one_hot) * one_hot, axis=1)
    destination = flat_expert * capacity + ranking
    flat_token = jnp.repeat(jnp.arange(tok_rows, dtype=jnp.int32), choices_count)
    outbox = (
        jnp.zeros((devices * capacity, width), jnp.bfloat16).at[destination].set(normed[flat_token])
    )
    outbox = outbox.reshape(devices, capacity, width)
    received = lax.all_to_all(outbox, EP, split_axis=0, concat_axis=0, tiled=True)
    served = apply_expert(received.reshape(-1, width), w_gate, w_up, w_down).reshape(received.shape)
    returned = exchange_by_chip(served, ("ep_0", "ep_1"), (1, 0), 0, 0)
    gathered_rows = returned.reshape(devices * capacity, width)[destination].reshape(
        tok_rows, choices_count, width
    )
    mixture = jnp.einsum("tk,tkd->td", gate_weights, gathered_rows.astype(jnp.float32))
    return normalize(mixture, post_gain).astype(jnp.bfloat16)


def solution(mesh):
    split = Mesh(mesh.devices.reshape(mesh.shape["grp"], 32, 2), ("grp", "ep_0", "ep_1"))
    placed = (
        P(GRP_EP, None),
        P(GRP_EP, None),
        P(GRP_EP, None),
        P(),
        P(EP, None, None),
        P(EP, None, None),
        P(EP, None, None),
        P(),
    )
    return jax.shard_map(
        body, mesh=split, in_specs=placed, out_specs=P(GRP_EP, None), check_vma=False
    )
```

profile of v0, /device:TPU:37, one launch (start us, length us, event | category | flops | bytes accessed | tf_op | source)
XLA Modules:
  0.0 285.6 jit_solution(3358752602286723334)
XLA Ops:
  0.0 0.9 copy.14
  0.9 0.7 broadcast_multiply_fusion
  1.8 0.2 reduce_window_sum.11
  2.0 0.2 select_reduce_fusion
  2.3 1.0 fusion.21
  3.6 1.0 fusion.23
  4.6 3.4 %scatter_custom_fusion = bf16[256,2048]{1,0:T(8,128)(2,1)S(1)} fusion(s32[128]{0:T(128)S(1)} %fusion.29, bf16[32,2048]{1,0:T(8,128)(2,1)S(1)} %fusion.23, s32[1024]{0:T(1024)S(1)} %pad_clamp_fusion.1, bf16[]{:T(256)} %constant.9.clone.1), kind=kCustom, calls=%fused_computation.11 | custom fusion | bytes 1048578 | tf_op jit(solution)/shard_map/scatter | solution.py:66
  7.9 1.2 reshape.89
  9.2 141.7 %all_to_all.15 = bf16[64,4,2048]{2,1,0:T(4,128)(2,1)S(1)} all-to-all(bf16[64,4,2048]{2,1,0:T(4,128)(2,1)} %reshape.89), channel_id=1, replica_groups=mesh['grp'=4,'ep_0'=32,'ep_1'=2] {'ep_0','ep_1'}, dimensions={0} | all-to-all | bytes 2097152 | tf_op jit(solution)/shard_map/all_to_all | solution.py:69
  150.9 1.1 reshape.90
  152.0 3.5 %fusion.3 = f32[256,512]{1,0:T(8,128)} fusion(bf16[256,2048]{1,0:T(8,128)(2,1)} %reshape.90, bf16[1,2048,512]{2,1,0:T(8,128)(2,1)} %param.12), kind=kOutput, calls=%fused_computation.7 | convolution fusion | flops 536870912 | bytes 3670016 | tf_op jit(solution)/shard_map/dot_general | solution.py:46
  155.5 4.0 %convolution_convert_fusion = bf16[256,2048]{1,0:T(8,128)(2,1)} fusion(bf16[1,512,2048]{2,1,0:T(8,128)(2,1)S(1)} %copy-done, bf16[256,2048]{1,0:T(8,128)(2,1)S(1)} %copy-done.1, bf16[1,2048,512]{2,1,0:T(8,128)(2,1)} %param.13, f32[256,512]{1,0:T(8,128)} %fusion.3), kind=kOutput, calls=%fused_computation.3 | convolution fusion | flops 1075052544 | bytes 6815744 | tf_op jit(solution)/shard_map/dot_general | solution.py:49
  159.6 1.5 reshape_reshape_reshape.6
  161.0 0.5 copy.15
  161.5 7.3 %all_to_all.16 = bf16[32,2,1,4,2048]{4,3,0,2,1:T(4,128)(2,1)S(1)} all-to-all(bf16[32,2,1,4,2048]{4,3,0,2,1:T(4,128)(2,1)S(1)} %copy.15), channel_id=1, replica_groups=mesh['grp'=4,'ep_0'=32,'ep_1'=2] {'ep_1'}, dimensions={1} | all-to-all | bytes 2097152 | tf_op jit(solution)/shard_map/all_to_all | solution.py:30
  168.8 1.5 copy.16
  170.3 5.5 %all-to-all-start.2 = ((bf16[32,2,1,4,2048]{4,3,1,2,0:T(4,128)(2,1)}), bf16[32,2,1,4,2048]{4,3,1,2,0:T(4,128)(2,1)}, u32[]{:S(2)}, u32[]{:S(2)}) async-start(bf16[32,2,1,4,2048]{4,3,1,2,0:T(4,128)(2,1)} %copy.16), calls=%async_computation.2 | async-start | bytes 2097152 | tf_op jit(solution)/shard_map/all_to_all | solution.py:30
  175.9 104.0 %all-to-all-done.2 = bf16[32,2,1,4,2048]{4,3,1,2,0:T(4,128)(2,1)} async-done(((bf16[32,2,1,4,2048]{4,3,1,2,0:T(4,128)(2,1)}), bf16[32,2,1,4,2048]{4,3,1,2,0:T(4,128)(2,1)}, u32[]{:S(2)}, u32[]{:S(2)}) %all-to-all-start.2) | async-done | bytes 1048608 | tf_op jit(solution)/shard_map/all_to_all | solution.py:30
  279.9 1.3 reshape_reshape_reshape.7
  281.2 1.7 gather_fusion
  283.0 1.2 reshape.91
  284.2 0.4 fusion.32
  284.6 0.2 fusion.24
  284.8 0.8 fusion.26
  (21 shorter events, 0.7 us)
Async XLA Ops:
  0.0 155.5 %copy-start = (bf16[1,512,2048]{2,1,0:T(8,128)(2,1)S(1)}, bf16[1,512,2048]{2,1,0:T(8,128)(2,1)}, u32[]{:S(2)}) copy-start(bf16[1,512,2048]{2,1,0:T(8,128)(2,1)} %param.14) | copy-start | bytes 6291460
  152.0 3.5 %copy-start.1 = (bf16[256,2048]{1,0:T(8,128)(2,1)S(1)}, bf16[256,2048]{1,0:T(8,128)(2,1)}, u32[]{:S(2)}) copy-start(bf16[256,2048]{1,0:T(8,128)(2,1)} %reshape.90) | copy-start | bytes 3145732
  168.8 7.0 %copy-start.3 = (f32[32,4]{0,1:T(4,128)S(1)}, f32[32,4]{0,1:T(4,128)}, u32[]{:S(2)}) copy-start(f32[32,4]{0,1:T(4,128)} %param.10) | copy-start | bytes 1540
  170.3 109.6 %all-to-all-start.2 = ((bf16[32,2,1,4,2048]{4,3,1,2,0:T(4,128)(2,1)}), bf16[32,2,1,4,2048]{4,3,1,2,0:T(4,128)(2,1)}, u32[]{:S(2)}, u32[]{:S(2)}) async-start(bf16[32,2,1,4,2048]{4,3,1,2,0:T(4,128)(2,1)} %copy.16), calls=%async_computation.2 | async-start | bytes 2097152 | tf_op jit(solution)/shard_map/all_to_all | solution.py:30
  283.0 1.9 copy-start.2
where the time goes:
time: 291 us; the launch traced here: 286 us
  blocking collectives  149 us (51%)
  waiting for transfers between devices  104 us (36%)
  local copies, waits for them, and re-layouts  14.8 us (5%)
  matrix products  7.95 us (3%)
  starting transfers between devices  5.46 us (2%)
  other arithmetic  4.14 us (1%)
    all_to_all x1, blocking collectives, body(): lax.all_to_all(outbox, EP, split_axis=0, concat_axis=0, tiled=True)  142 us
    all_to_all x1, waiting for transfers between devices, exchange_in_order(): lax.all_to_all(tiles, axes[k], split_axis=k, concat_axis=k, tiled=True)  104 us
    all_to_all x1, blocking collectives, exchange_in_order(): lax.all_to_all(tiles, axes[k], split_axis=k, concat_axis=k, tiled=True)  7.28 us
  transfers between devices with their start and end apart: 1, of which 1 were waited for; matrix products, arithmetic and copies ran while one was open for 0% of the time, Pallas kernels for 0%

commit v1 on v0

v1 whole, which is shorter than its diff:
```python
import jax
import jax.numpy as jnp
from jax import lax
from jax.sharding import Mesh
from jax.sharding import PartitionSpec as P

SET = 8
TAIL = 128
EP = ("set", "mem")
ALL = ("grp", "set", "mem")

epsilon = 1e-06


def normalize(values, gain):
    floats = values.astype(jnp.float32)
    return floats * lax.rsqrt(jnp.mean(floats * floats, axis=-1, keepdims=True) + epsilon) * gain


def body(tokens, routing, gate_weights, pre_gain, w_gate, w_up, w_down, post_gain):
    normed = normalize(tokens, pre_gain).astype(jnp.bfloat16)
    tok_rows, width = tokens.shape
    sets = lax.axis_size("set")
    slots = sets * SET
    own_set = routing[:, 0] // SET
    same = (own_set[:, None] == own_set[None, :]) & (
        jnp.arange(tok_rows)[:, None] > jnp.arange(tok_rows)[None, :]
    )
    slot = own_set * SET + jnp.sum(same.astype(jnp.int32), axis=1)
    place = slot[None, :] == jnp.arange(slots)[:, None]
    member = routing % SET
    weights = jnp.sum(
        jnp.where(member[:, :, None] == jnp.arange(SET), gate_weights[:, :, None], 0.0), axis=1
    )
    high = weights.astype(jnp.bfloat16)
    low = (weights - high.astype(jnp.float32)).astype(jnp.bfloat16)
    tail = jnp.concatenate([high, low, jnp.zeros((tok_rows, TAIL - 2 * SET), jnp.bfloat16)], axis=1)
    rows = jnp.concatenate([normed, tail], axis=1)
    outbox = jnp.dot(
        place.astype(jnp.bfloat16), rows, preferred_element_type=jnp.float32
    ).astype(jnp.bfloat16)
    entered = lax.all_to_all(outbox, EP, split_axis=0, concat_axis=0, tiled=True)
    shared = lax.all_gather(entered, "mem", axis=0, tiled=True)
    x = shared[:, :width]
    mine = (jnp.arange(SET) == lax.axis_index("mem")).astype(jnp.float32)
    weight = jnp.sum(
        (
            shared[:, width : width + SET].astype(jnp.float32)
            + shared[:, width + SET : width + 2 * SET].astype(jnp.float32)
        )
        * mine,
        axis=1,
        keepdims=True,
    )
    gate = jnp.dot(x, w_gate[0], preferred_element_type=jnp.float32)
    upward = jnp.dot(x, w_up[0], preferred_element_type=jnp.float32)
    hidden = (jax.nn.silu(gate) * upward).astype(jnp.bfloat16)
    out = jnp.dot(hidden, w_down[0], preferred_element_type=jnp.float32)
    part = (out.astype(jnp.bfloat16).astype(jnp.float32) * weight).astype(jnp.bfloat16)
    summed = lax.psum_scatter(part, "mem", scatter_dimension=0, tiled=True)
    home = lax.all_to_all(summed, EP, split_axis=0, concat_axis=0, tiled=True)
    mixture = jnp.dot(
        place.T.astype(jnp.bfloat16), home, preferred_element_type=jnp.float32
    )
    return normalize(mixture, post_gain).astype(jnp.bfloat16)


def solution(mesh):
    ep = mesh.shape["ep"]
    split = Mesh(mesh.devices.reshape(mesh.shape["grp"], ep // SET, SET), ALL)
    placed = (
        P(ALL, None),
        P(ALL, None),
        P(ALL, None),
        P(),
        P(EP, None, None),
        P(EP, None, None),
        P(EP, None, None),
        P(),
    )
    return jax.shard_map(
        body, mesh=split, in_specs=placed, out_specs=P(ALL, None), check_vma=False
    )
```

time: 291 us -> 265 us (0.911); the launches traced: 286 us -> 264 us
  waiting for transfers between devices: 104 us -> 85.8 us
  between operations: 0.14 us -> 13.5 us
  local copies, waits for them, and re-layouts: 14.8 us -> 3.82 us
  blocking collectives: 149 us -> 142 us
  starting transfers between devices: 5.46 us -> 0.07 us
  other arithmetic: 4.14 us -> 9.16 us
    all_to_all x1 -> x0, waiting for transfers between devices: 104 us -> none  [exchange_in_order(): lax.all_to_all(tiles, axes[k], split_axis=k, concat_axis=k, tiled=True)]
    all_to_all x1, blocking collectives: 142 us -> 77.2 us  [body(): lax.all_to_all(outbox, EP, split_axis=0, concat_axis=0, tiled=True)]
    all_to_all x1, blocking collectives: 7.28 us -> 64.5 us  [body(): home = lax.all_to_all(summed, EP, split_axis=0, concat_axis=0, tiled=True)]
    reduce_scatter x0 -> x1, waiting for transfers between devices: none -> 52.3 us  [body(): summed = lax.psum_scatter(part, 'mem', scatter_dimension=0, tiled=True)]
    all_gather x0 -> x1, waiting for transfers between devices: none -> 33.4 us  [body(): shared = lax.all_gather(entered, 'mem', axis=0, tiled=True)]
    all_to_all x1 -> x0, starting transfers between devices: 5.46 us -> none  [exchange_in_order(): lax.all_to_all(tiles, axes[k], split_axis=k, concat_axis=k, tiled=True)]
    reshape x4 -> x0, local copies, waits for them, and re-layouts: 3.7 us -> none  [the longest x1 1.25 us: body(): returned.reshape(devices * capacity, width)[destination]]
    scatter x1 -> x0, local copies, waits for them, and re-layouts: 3.36 us -> none  [body(): jnp.zeros((devices * capacity, width), jnp.bfloat16).at[destination]]
  transfers between devices with their start and end apart: 1 -> 2, of which waited for: 1 -> 2; matrix products, arithmetic and copies ran while one was open for 0% -> 0% of each run, Pallas kernels for 0% -> 0%
where the time goes in v1:
time: 265 us; the launch traced here: 264 us
  blocking collectives  142 us (54%)
  waiting for transfers between devices  85.8 us (32%)
  between operations  13.5 us (5%)
  matrix products  10.1 us (4%)
  other arithmetic  9.16 us (3%)
  local copies, waits for them, and re-layouts  3.82 us (1%)
    all_to_all x1, blocking collectives, body(): lax.all_to_all(outbox, EP, split_axis=0, concat_axis=0, tiled=True)  77.2 us
    all_to_all x1, blocking collectives, body(): home = lax.all_to_all(summed, EP, split_axis=0, concat_axis=0, tiled=True)  64.5 us
    reduce_scatter x1, waiting for transfers between devices, body(): summed = lax.psum_scatter(part, 'mem', scatter_dimension=0, tiled=True)  52.3 us
    all_gather x1, waiting for transfers between devices, body(): shared = lax.all_gather(entered, 'mem', axis=0, tiled=True)  33.4 us
    dot_general x1, matrix products, body(): out = jnp.dot(hidden, w_down[0], preferred_element_type=jnp.float32)  6 us
  transfers between devices with their start and end apart: 2, of which 2 were waited for; matrix products, arithmetic and copies ran while one was open for 0% of the time, Pallas kernels for 0%

profile of v1, /device:TPU:37, one launch (start us, length us, event | category | flops | bytes accessed | tf_op | source)
XLA Modules:
  0.0 264.2 jit_solution(17228135809139778292)
XLA Ops:
  6.6 0.8 fusion.33
  7.4 0.7 and_select_fusion.1
  8.1 0.7 add_select_fusion
  8.8 1.0 fusion.23
  10.0 0.7 multiply_add_fusion
  10.7 0.7 select_reduce_fusion
  11.6 1.0 fusion.25
  12.7 0.2 fusion
  12.9 0.5 broadcast.123
  13.4 0.8 reduce
  14.2 0.3 reshape.72
  14.5 77.2 %all_to_all.24 = bf16[64,2,1088]{2,1,0:T(2,128)(2,1)S(1)} all-to-all(bf16[64,2,1088]{2,1,0:T(2,128)(2,1)S(1)} %reshape.72), channel_id=1, replica_groups=mesh['grp'=4,'set'=8,'mem'=8] {'set','mem'}, dimensions={0} | all-to-all | bytes 557056 | tf_op jit(solution)/shard_map/all_to_all | solution.py:42
  91.7 0.3 reshape.73
  92.1 0.7 copy.28
  93.0 33.4 %all-gather.3.cloned.1.call-done = bf16[512,1,2176]{2,0,1:T(8,128)(2,1)} async-done(((bf16[64,1,2176]{2,0,1:T(8,128)(2,1)}), bf16[512,1,2176]{2,0,1:T(8,128)(2,1)}) %all-gather.3.cloned.1.call-update) | async-done | bytes 2228240 | tf_op jit(solution)/shard_map/all_gather | solution.py:43
  126.4 1.1 fusion.35
  127.6 3.5 %fusion.4 = f32[512,512]{1,0:T(8,128)S(1)} fusion(bf16[1,2048,512]{2,1,0:T(8,128)(2,1)} %param.12, bf16[512,2176]{1,0:T(8,128)(2,1)} %bitcast.39), kind=kOutput, calls=%fused_computation.7 | convolution fusion | flops 1073741824 | bytes 5242880 | tf_op jit(solution)/shard_map/dot_general | solution.py:55
  131.2 6.0 %multiply_convert_fusion = bf16[512,2048]{1,0:T(8,128)(2,1)} fusion(bf16[1,512,2048]{2,1,0:T(8,128)(2,1)S(1)} %copy-done, f32[512]{0:T(512)S(1)} %multiply_reduce_fusion.1, bf16[1,2048,512]{2,1,0:T(8,128)(2,1)} %param.13, bf16[512,2176]{1,0:T(8,128)(2,1)} %bitcast.40, f32[512,512]{1,0:T(8,128)S(1)} %fusion.4), kind=kOutput, calls=%fused_computation | convolution fusion | flops 2153250816 | bytes 9439232 | tf_op jit(solution)/shard_map/dot_general | solution.py:58
  137.3 52.3 %reduce-scatter.2.cloned.1.call-done = bf16[64,2048]{1,0:T(8,128)(2,1)} async-done(((bf16[512,2048]{1,0:T(8,128)(2,1)}), bf16[64,2048]{1,0:T(8,128)(2,1)}) %reduce-scatter.2.cloned.1.call-update) | async-done | bytes 262160 | tf_op jit(solution)/shard_map/reduce_scatter | solution.py:60
  189.6 1.7 reduce.1
  191.5 64.5 %all_to_all.25 = bf16[64,2,1024]{2,1,0:T(2,128)(2,1)S(1)} all-to-all(bf16[64,2,1024]{2,1,0:T(2,128)(2,1)S(1)} %reshape.74), channel_id=1, replica_groups=mesh['grp'=4,'set'=8,'mem'=8] {'set','mem'}, dimensions={0} | all-to-all | bytes 524288 | tf_op jit(solution)/shard_map/all_to_all | solution.py:61
  256.0 0.2 reshape.75
  256.2 0.4 multiply_reduce_fusion
  256.6 0.8 multiply_convert_fusion.1
  (21 shorter events, 1.1 us)
Async XLA Ops:
  6.5 124.7 %copy-start = (bf16[1,512,2048]{2,1,0:T(8,128)(2,1)S(1)}, bf16[1,512,2048]{2,1,0:T(8,128)(2,1)}, u32[]{:S(2)}) copy-start(bf16[1,512,2048]{2,1,0:T(8,128)(2,1)} %param.14) | copy-start | bytes 6291460
  6.6 119.8 %all-gather.3.cloned.1.call-start = ((), (), s32[]{:S(2)}) async-start(), calls=%async_computation.4 | async-start | bytes 2506752 | tf_op jit(solution)/shard_map/all_gather | solution.py:43
  92.9 96.7 %reduce-scatter.2.cloned.1.call-start = ((), (), s32[]{:S(2)}) async-start(), calls=%async_computation.3 | async-start | bytes 2359296 | tf_op jit(solution)/shard_map/reduce_scatter | solution.py:60
  137.2 119.4 %copy-start.1 = (f32[2048]{0:T(1024)S(1)}, f32[2048]{0:T(1024)}, u32[]{:S(2)}) copy-start(f32[2048]{0:T(1024)} %param.15) | copy-start | bytes 24580
Sparse Core Ops, SparseCore 0:
  93.0 33.3 all-gather.2
  137.4 52.1 reduce-scatter.1
